TPU v7x, 32 devices: a whole 2x2x4 slice. The times are simulated.
32 devices in a mesh: sp: 8 (over z, y), tp: 4 (over x, core).
Axes of the slice: x: 2, y: 2, z: 4, core: 2. Of those that a mesh axis runs over, the one named last changes fastest.
Arguments:
- queries: bfloat16 [4096, 1024], P('sp', 'tp'), may hold values from -60 to 60
- keys: bfloat16 [4096, 1024], P('sp', 'tp'), may hold values from -6 to 6
- values: bfloat16 [4096, 1024], P('sp', 'tp'), may hold values from -6 to 6
- lambdas: float32 [8], P('tp'), may hold values from 0.3 to 0.8
- head_gain: float32 [128], replicated, may hold values from 0.1 to 1.9
- w_out: bfloat16 [1024, 2048], replicated, may hold values from -0.1875 to 0.1875
- residual_in: bfloat16 [4096, 2048], P(('sp', 'tp')), may hold values from -6 to 6
- norm_gain: float32 [2048], replicated, may hold values from 0.1 to 1.9
- route_ids: int32 [4096, 2], P(('sp', 'tp')), may hold values from 0 to 7, as said below
- route_weight: float32 [4096, 2], P(('sp', 'tp')), may hold values from 0.2 to 1
- w_gate: bfloat16 [8, 2048, 1024], P('sp', None, 'tp'), may hold values from -0.125 to 0.125
- w_up: bfloat16 [8, 2048, 1024], P('sp', None, 'tp'), may hold values from -0.125 to 0.125
- w_down: bfloat16 [8, 2048, 1024], P('sp', None, 'tp'), may hold values from -0.1875 to 0.1875
Outputs:
- layer_out: bfloat16 [4096, 2048], P(('sp', 'tp'))
Inputs may be any that keep to these rules, and one draw needn't show every extreme that they name: `route_ids`: each row names two different experts of one group (the same expert // 8). Among the 128 rows of one device (aligned blocks), no expert is named more than 64 times, and in every draw one expert is named exactly 64 times in the rows of every device.
All inputs are finite; a program needn't handle non-finite values.
Results may differ from a plain program's by a relative error of at most 0.015.
Values may be sent and summed in bfloat16 or wider, within the bound.
A program may use at most 128 MiB of HBM per device.

v0:
```python
import functools
import math

import jax
import jax.numpy as jnp
from jax import lax
from jax.experimental import pallas as pl
from jax.experimental.pallas import tpu as pltpu
from jax.sharding import PartitionSpec as P

EPSILON = 1e-06
OUT_SCALE = 0.8
FLOOR_SCORE = -1e30


def swapped(value, axis, distance):
    mask = 2**distance
    pairs = [(source, source ^ mask) for source in range(lax.axis_size(axis))]
    return lax.ppermute(value, axis, pairs)


def slot_numbers(flat_ids):
    count_ids = flat_ids.shape[0]
    positions = lax.broadcasted_iota(jnp.int32, (count_ids, count_ids), 0)
    earlier = lax.broadcasted_iota(jnp.int32, (count_ids, count_ids), 1) < positions
    matches = (flat_ids[:, None] == flat_ids[None, :]) & earlier
    return jnp.sum(matches.astype(jnp.int32), axis=1)


def send_back(results):
    return lax.all_to_all(results, "sp", split_axis=0, concat_axis=0, tiled=True)

MESH = pl.DeviceIdType.MESH
VMEM_BYTES = 60 * 1024 * 1024


def ring_neighbours(group):
    me = lax.axis_index("sp")
    spot = lax.rem(me, group)
    base = me - spot
    even = lax.rem(spot, 2) == 0
    up = jnp.where(even, jnp.where(spot == group - 2, group - 1, spot + 2), jnp.where(spot == 1, 0, spot - 2))
    down = jnp.where(even, jnp.where(spot == 0, 1, spot - 2), jnp.where(spot == group - 1, group - 2, spot + 2))
    return base + up, base + down


def attention_kernel(
    group,
    tp,
    q_ref,
    k_ref,
    v_ref,
    lam_ref,
    gain_ref,
    w_out_ref,
    residual_ref,
    norm_gain_ref,
    gate_ref,
    up_ref,
    carried_ref,
    normed_ref,
    far_gate_ref,
    far_up_ref,
    k_slots,
    v_slots,
    q_masked,
    peaks,
    totals,
    numerators,
    made,
    came,
    w_out_here,
    send_sems,
    recv_sems,
    row_send,
    row_recv,
    load_sems,
    far_send,
    far_recv,
):
    rows = q_ref.shape[0]
    heads = lam_ref.shape[0]
    value_dim = v_ref.shape[1] // heads
    head_dim = value_dim // 2
    exponent_scale = head_dim ** (-0.5) * math.log2(math.e)
    right, left = ring_neighbours(group)
    me_tp = lax.axis_index("tp")

    barrier = pltpu.get_barrier_semaphore()
    for neighbour in (right, left):
        pl.semaphore_signal(barrier, inc=1, device_id={"sp": neighbour}, device_id_type=MESH)
    for step in range(1, tp):
        pl.semaphore_signal(
            barrier, inc=1, device_id={"tp": lax.rem(me_tp + step, tp)}, device_id_type=MESH
        )
    pl.semaphore_wait(barrier, 2 + tp - 1)

    def send(source, slots, which, slot, target):
        return pltpu.make_async_remote_copy(
            src_ref=source,
            dst_ref=slots.at[slot],
            send_sem=send_sems.at[which, slot],
            recv_sem=recv_sems.at[which, slot],
            device_id={"sp": target},
            device_id_type=MESH,
        )

    last = group - 1
    if group > 2:
        for slot, target in ((1, right), (2, left)):
            send(k_ref, k_slots, 0, slot, target).start()
            send(v_ref, v_slots, 1, slot, target).start()
    elif group == 2:
        send(k_ref, k_slots, 0, 1, right).start()
        send(v_ref, v_slots, 1, 1, left).start()
    own_loads = (
        pltpu.make_async_copy(k_ref, k_slots.at[0], load_sems.at[0]),
        pltpu.make_async_copy(v_ref, v_slots.at[0], load_sems.at[1]),
    )
    for load in own_loads:
        load.start()
    load_w_out = pltpu.make_async_copy(w_out_ref, w_out_here, load_sems.at[2])
    load_w_out.start()

    far_copies = [
        pltpu.make_async_remote_copy(
            src_ref=source,
            dst_ref=landing,
            send_sem=far_send.at[index],
            recv_sem=far_recv.at[index],
            device_id={"tp": lax.rem(me_tp + tp // 2, tp)},
            device_id_type=MESH,
        )
        for index, (source, landing) in enumerate(((gate_ref, far_gate_ref), (up_ref, far_up_ref)))
    ]
    for copy in far_copies:
        copy.start()

    lane = lax.broadcasted_iota(jnp.int32, (rows, value_dim), 1)
    for head in range(heads):
        both = q_ref[:, head * value_dim : (head + 1) * value_dim]
        q_masked[2 * head] = jnp.where(lane < head_dim, both, jnp.zeros_like(both))
        q_masked[2 * head + 1] = jnp.where(lane >= head_dim, both, jnp.zeros_like(both))
    peaks[...] = jnp.full(peaks.shape, FLOOR_SCORE, jnp.float32)
    totals[...] = jnp.zeros(totals.shape, jnp.float32)
    numerators[...] = jnp.zeros(numerators.shape, jnp.float32)
    for load in own_loads:
        load.wait()

    chunk = min(rows, 256)

    def absorb(slot, count):
        keys_here = count * k_slots.shape[1]
        for head in range(heads):
            columns = slice(head * value_dim, (head + 1) * value_dim)
            key_block = k_slots[pl.ds(slot, count), :, columns].reshape(keys_here, value_dim)
            value_block = v_slots[pl.ds(slot, count), :, columns].reshape(keys_here, value_dim)
            with_ones = jnp.concatenate(
                [value_block, jnp.ones((keys_here, 128), jnp.bfloat16)], axis=1
            )
            for part in (2 * head, 2 * head + 1):
                for begin in range(0, rows, chunk):
                    here = slice(begin, begin + chunk)
                    scores = lax.dot_general(
                        q_masked[part, here],
                        key_block,
                        (((1,), (1,)), ((), ())),
                        preferred_element_type=jnp.float32,
                    )
                    old_peak = peaks[part, here][:, :1]
                    new_peak = jnp.maximum(old_peak, jnp.max(scores, axis=1, keepdims=True))
                    weights = jnp.exp2((scores - new_peak) * exponent_scale)
                    shrink = jnp.exp2((old_peak - new_peak) * exponent_scale)
                    product = jnp.dot(
                        weights.astype(jnp.bfloat16), with_ones, preferred_element_type=jnp.float32
                    )
                    numerators[part, here] = (
                        numerators[part, here] * shrink + product[:, :value_dim]
                    )
                    totals[part, here] = totals[part, here] * shrink + product[:, value_dim:]
                    peaks[part, here] = jnp.broadcast_to(new_peak, (chunk, 128))

    def one_pair(pair, unused):
        slot = 2 * pair + 1

        def pass_on(which, slots, at, target):
            send(slots.at[at], slots, which, at, target).wait_recv()

            @pl.when(at + 2 <= last - 1)
            def _():
                send(slots.at[at], slots, which, at + 2, target).start()

        for which, slots in ((0, k_slots), (1, v_slots)):
            pass_on(which, slots, slot, right)
            if which == 0:

                @pl.when(slot == last - 2)
                def _():
                    send(slots.at[slot], slots, which, last, right).start()

            pass_on(which, slots, slot + 1, left)
            if which == 1:

                @pl.when(slot == last - 2)
                def _():
                    send(slots.at[slot + 1], slots, which, last, left).start()

        absorb(slot, 2)
        return unused

    absorb(0, 1)
    lax.fori_loop(0, (group - 2) // 2, one_pair, 0)
    if last:
        send(k_slots.at[last], k_slots, 0, last, right).wait_recv()
        send(v_slots.at[last], v_slots, 1, last, left).wait_recv()
        absorb(last, 1)

    gain = gain_ref[...] * OUT_SCALE
    for head in range(heads):
        first = numerators[2 * head] / totals[2 * head][:, :1]
        second = numerators[2 * head + 1] / totals[2 * head + 1][:, :1]
        combined = first - lam_ref[head] * second
        mean_square = jnp.mean(combined * combined, axis=1, keepdims=True)
        made[:, head * value_dim : (head + 1) * value_dim] = (
            combined * lax.rsqrt(mean_square + EPSILON) * gain
        ).astype(jnp.bfloat16)

    dev_rows = residual_ref.shape[0]

    def row_copy(step, owner, target):
        return pltpu.make_async_remote_copy(
            src_ref=made.at[pl.ds(pl.multiple_of(target * dev_rows, dev_rows), dev_rows)],
            dst_ref=came.at[owner],
            send_sem=row_send.at[step],
            recv_sem=row_recv.at[step],
            device_id={"tp": target},
            device_id_type=MESH,
        )

    sends = [row_copy(step, me_tp, lax.rem(me_tp + step, tp)) for step in range(1, tp)]
    for copy in sends:
        copy.start()
    came[me_tp] = made[pl.ds(pl.multiple_of(me_tp * dev_rows, dev_rows), dev_rows)]
    load_w_out.wait()
    for step in range(1, tp):
        row_copy(
            step, lax.rem(me_tp + tp - step, tp), lax.rem(me_tp + step, tp)
        ).wait_recv()
    attended = jnp.concatenate([came[peer] for peer in range(tp)], axis=1)
    mixed = jnp.dot(attended, w_out_here[...], preferred_element_type=jnp.float32).astype(
        jnp.bfloat16
    )
    carried = (residual_ref[...].astype(jnp.float32) + mixed.astype(jnp.float32)).astype(
        jnp.bfloat16
    )
    carried_ref[...] = carried
    wide = carried.astype(jnp.float32)
    spread = jnp.mean(wide * wide, axis=1, keepdims=True)
    normed_ref[...] = (wide * lax.rsqrt(spread + EPSILON) * norm_gain_ref[...]).astype(
        jnp.bfloat16
    )
    for copy in sends:
        copy.wait_send()
    for slot in range(1, group):
        send(k_ref, k_slots, 0, slot, right).wait_send()
        send(v_ref, v_slots, 1, slot, right).wait_send()
    for copy in far_copies:
        copy.wait()


def attend(queries, keys, values, lambdas, head_gain, w_out, residual_in, norm_gain, gate, up):
    group = min(16, lax.axis_size("sp"))
    tp = lax.axis_size("tp")
    rows, width = queries.shape
    dev_rows, model_width = residual_in.shape
    heads = lambdas.shape[0]
    value_dim = width // heads
    vmem = pl.BlockSpec(memory_space=pltpu.VMEM)
    return pl.pallas_call(
        functools.partial(attention_kernel, group, tp),
        name="attend",
        out_shape=(
            jax.ShapeDtypeStruct((dev_rows, model_width), jnp.bfloat16),
            jax.ShapeDtypeStruct((dev_rows, model_width), jnp.bfloat16),
            jax.ShapeDtypeStruct(gate.shape, jnp.bfloat16),
            jax.ShapeDtypeStruct(up.shape, jnp.bfloat16),
        ),
        in_specs=[
            vmem,
            vmem,
            vmem,
            pl.BlockSpec(memory_space=pltpu.SMEM),
            vmem,
            pl.BlockSpec(memory_space=pl.ANY),
            vmem,
            vmem,
            pl.BlockSpec(memory_space=pl.ANY),
            pl.BlockSpec(memory_space=pl.ANY),
        ],
        out_specs=(
            vmem,
            vmem,
            pl.BlockSpec(memory_space=pl.ANY),
            pl.BlockSpec(memory_space=pl.ANY),
        ),
        scratch_shapes=[
            pltpu.VMEM((group, rows, width), jnp.bfloat16),
            pltpu.VMEM((group, rows, width), jnp.bfloat16),
            pltpu.VMEM((2 * heads, rows, value_dim), jnp.bfloat16),
            pltpu.VMEM((2 * heads, rows, 128), jnp.float32),
            pltpu.VMEM((2 * heads, rows, 128), jnp.float32),
            pltpu.VMEM((2 * heads, rows, value_dim), jnp.float32),
            pltpu.VMEM((rows, width), jnp.bfloat16),
            pltpu.VMEM((tp, dev_rows, width), jnp.bfloat16),
            pltpu.VMEM(w_out.shape, jnp.bfloat16),
            pltpu.SemaphoreType.DMA((2, group)),
            pltpu.SemaphoreType.DMA((2, group)),
            pltpu.SemaphoreType.DMA((tp,)),
            pltpu.SemaphoreType.DMA((tp,)),
            pltpu.SemaphoreType.DMA((3,)),
            pltpu.SemaphoreType.DMA((2,)),
            pltpu.SemaphoreType.DMA((2,)),
        ],
        compiler_params=pltpu.CompilerParams(
            collective_id=0, has_side_effects=True, vmem_limit_bytes=VMEM_BYTES
        ),
        cost_estimate=pl.CostEstimate(
            flops=50_000_000_000, bytes_accessed=16_000_000, transcendentals=8_000_000
        ),
    )(
        queries,
        keys,
        values,
        lambdas,
        head_gain.reshape(1, -1),
        w_out,
        residual_in,
        norm_gain.reshape(1, -1),
        gate,
        up,
    )


def expert_kernel(
    group,
    x_ref,
    carried_ref,
    share_ref,
    gate_ref,
    up_ref,
    down_ref,
    far_gate_ref,
    far_up_ref,
    out_ref,
    x_slots,
    share_slots,
    gates,
    ups,
    downs,
    hidden,
    parts,
    sums_in,
    sums_out,
    send_sems,
    recv_sems,
    sum_send,
    sum_recv,
    load_sems,
    weight_send,
    weight_recv,
):
    rows, width = x_ref.shape
    pieces = gates.shape[0]
    half_rows, half_width = rows // 2, width // 2
    last, half = group - 1, group // 2
    right, left = ring_neighbours(group)
    expert = lax.axis_index("sp")
    me_tp = lax.axis_index("tp")
    near = me_tp + 1 - 2 * lax.rem(me_tp, 2)
    far = lax.rem(me_tp + pieces // 2, pieces)

    barrier = pltpu.get_barrier_semaphore()
    for neighbour in (right, left):
        pl.semaphore_signal(barrier, inc=1, device_id={"sp": neighbour}, device_id_type=MESH)
    for neighbour in (near, far):
        pl.semaphore_signal(barrier, inc=1, device_id={"tp": neighbour}, device_id_type=MESH)
    pl.semaphore_wait(barrier, 4)

    def landing(slot, which):
        return share_slots.at[slot] if which == 2 else x_slots.at[slot, which]

    def send(source, slot, which, target):
        return pltpu.make_async_remote_copy(
            src_ref=source,
            dst_ref=landing(slot, which),
            send_sem=send_sems.at[which, slot],
            recv_sem=recv_sems.at[which, slot],
            device_id={"sp": target},
            device_id_type=MESH,
        )

    def weight_send_to(source, target_ref, index, target):
        return pltpu.make_async_remote_copy(
            src_ref=source,
            dst_ref=target_ref,
            send_sem=weight_send.at[index],
            recv_sem=weight_recv.at[index],
            device_id={"tp": target},
            device_id_type=MESH,
        )

    own = (x_ref.at[pl.ds(0, half_rows)], x_ref.at[pl.ds(half_rows, half_rows)], share_ref)
    for which in range(3):
        send(own[which], 1, which, right).start()
        send(own[which], 2, which, left).start()
    far_down = weight_send_to(down_ref, downs.at[2], 5, far)
    far_down.start()
    near_copies = [
        weight_send_to(gate_ref, gates.at[1], 0, near),
        weight_send_to(far_gate_ref, gates.at[3], 1, near),
        weight_send_to(up_ref, ups.at[1], 2, near),
        weight_send_to(far_up_ref, ups.at[3], 3, near),
        weight_send_to(down_ref, downs.at[1], 4, near),
    ]
    loads = [
        pltpu.make_async_copy(gate_ref, gates.at[0], load_sems.at[0]),
        pltpu.make_async_copy(up_ref, ups.at[0], load_sems.at[1]),
        pltpu.make_async_copy(far_gate_ref, gates.at[2], load_sems.at[2]),
        pltpu.make_async_copy(far_up_ref, ups.at[2], load_sems.at[3]),
        pltpu.make_async_copy(down_ref, downs.at[0], load_sems.at[4]),
    ]
    for copy in near_copies + loads:
        copy.start()
    def make_hidden(x, begin):
        def one_piece(piece, unused):
            gate_proj = jnp.dot(x, gates[piece], preferred_element_type=jnp.float32)
            up_proj = jnp.dot(x, ups[piece], preferred_element_type=jnp.float32)
            silu = gate_proj / (1.0 + jnp.exp(-gate_proj))
            hidden[piece, begin : begin + x.shape[0]] = (silu * up_proj).astype(jnp.bfloat16)
            return unused

        lax.fori_loop(0, pieces, one_piece, 0)

    def share_column(share):
        wanted = lax.broadcasted_iota(jnp.int32, share.shape, 0) == expert
        line = jnp.sum(jnp.where(wanted, share, 0.0), axis=0, keepdims=True)
        down_index = lax.broadcasted_iota(jnp.int32, (rows, rows), 0)
        across_index = lax.broadcasted_iota(jnp.int32, (rows, rows), 1)
        square = jnp.where(down_index == across_index, jnp.broadcast_to(line, (rows, rows)), 0.0)
        return jnp.sum(square, axis=1, keepdims=True)

    tile = width // 4

    def make_parts(slots):
        begin, count = slots[0] * rows, len(slots) * rows
        columns = [share_column(share_ref[...] if slot == 0 else share_slots[slot]) for slot in slots]
        column = jnp.concatenate(columns, axis=0)

        def one_tile(index, unused):
            at = pl.ds(pl.multiple_of(index * tile, tile), tile)
            total = jnp.zeros((count, tile), jnp.float32)
            for piece in range(pieces):
                total = total + lax.dot_general(
                    hidden[piece, begin : begin + count],
                    downs[piece, at, :],
                    (((1,), (1,)), ((), ())),
                    preferred_element_type=jnp.float32,
                )
            parts[begin : begin + count, at] = total.astype(jnp.bfloat16).astype(jnp.float32) * column
            return unused

        lax.fori_loop(0, 4, one_tile, 0)

    def exchange(step):
        ahead, behind = 2 * step - 1, 2 * step
        for which in range(3):
            send(landing(ahead, which), ahead, which, right).wait_recv()
            if step < half - 1:
                send(landing(ahead, which), ahead + 2, which, right).start()
            elif which != 1:
                send(landing(ahead, which), last, which, right).start()
            send(landing(behind, which), behind, which, left).wait_recv()
            if step < half - 1:
                send(landing(behind, which), behind + 2, which, left).start()
            elif which == 1:
                send(landing(behind, which), last, which, left).start()

    def sum_copy(side, step, chunk):
        return pltpu.make_async_remote_copy(
            src_ref=sums_out.at[side, step, chunk],
            dst_ref=sums_in.at[side, step, chunk],
            send_sem=sum_send.at[side, step, chunk],
            recv_sem=sum_recv.at[side, step, chunk],
            device_id={"sp": left if side else right},
            device_id_type=MESH,
        )

    def part_of(side, slot, chunk):
        begin = slot * rows + chunk * half_rows
        return parts[begin : begin + half_rows, side * half_width : (side + 1) * half_width]

    def sum_step(step):
        for chunk in range(2):
            for side in range(2):
                if step < half:
                    slot = 2 * step - 1 + side
                elif step == half:
                    slot = last
                else:
                    slot = 2 * (group - step) - side
                value = part_of(side, slot, chunk)
                if step > 1:
                    sum_copy(side, step - 1, chunk).wait_recv()
                    value = value + sums_in[side, step - 1, chunk].astype(jnp.float32)
                sums_out[side, step, chunk] = value.astype(jnp.bfloat16)
                sum_copy(side, step, chunk).start()

    def pair_hidden(step):
        pair = jnp.concatenate(
            [x_slots[slot, part] for slot in (2 * step - 1, 2 * step) for part in range(2)], axis=0
        )
        make_hidden(pair, (2 * step - 1) * rows)

    exchange(1)
    for load in loads:
        load.wait()
    for copy in near_copies:
        copy.wait_recv()
    pair_hidden(1)
    if half > 2:
        exchange(2)
        pair_hidden(2)
    far_down.wait_recv()
    near_down = weight_send_to(downs.at[2], downs.at[3], 6, near)
    near_down.start()
    near_down.wait_recv()
    make_parts((1, 2))
    for step in range(3, half):
        exchange(step)
        sum_step(step - 2)
        make_parts((2 * step - 3, 2 * step - 2))
        pair_hidden(step)
    if half > 2:
        sum_step(half - 2)
        make_parts((last - 2, last - 1))
    send(landing(last, 0), last, 0, right).wait_recv()
    send(landing(last, 1), last, 1, left).wait_recv()
    send(landing(last, 2), last, 2, right).wait_recv()
    sum_step(half - 1)
    make_hidden(jnp.concatenate([x_slots[last, 0], x_slots[last, 1]], axis=0), last * rows)
    make_parts((last,))
    for step in range(half, group):
        sum_step(step)
        if step == half:
            make_hidden(x_ref[...], 0)
        if step == min(half + 1, last):
            make_parts((0,))
    for chunk in range(2):
        here = slice(chunk * half_rows, (chunk + 1) * half_rows)
        for side in range(2):
            there = slice(side * half_width, (side + 1) * half_width)
            sum_copy(side, last, chunk).wait_recv()
            out_ref[here, there] = (
                carried_ref[here, there].astype(jnp.float32)
                + (part_of(side, 0, chunk) + sums_in[side, last, chunk].astype(jnp.float32))
            ).astype(jnp.bfloat16)
    for slot in range(1, group):
        for which in range(3):
            send(landing(slot, which), slot, which, right).wait_send()
    for step in range(1, group):
        for side in range(2):
            for chunk in range(2):
                sum_copy(side, step, chunk).wait_send()
    for copy in near_copies + [far_down, near_down]:
        copy.wait_send()


def expert_layer(normed, carried, shares, gate, up, down, far_gate, far_up):
    group = lax.axis_size("sp")
    pieces = lax.axis_size("tp")
    rows, width = normed.shape
    units = gate.shape[1]
    vmem = pl.BlockSpec(memory_space=pltpu.VMEM)
    outside = pl.BlockSpec(memory_space=pl.ANY)
    bf16 = jnp.bfloat16
    return pl.pallas_call(
        functools.partial(expert_kernel, group),
        name="experts",
        out_shape=jax.ShapeDtypeStruct((rows, width), bf16),
        in_specs=[vmem] * 3 + [outside] * 5,
        out_specs=vmem,
        scratch_shapes=[
            pltpu.VMEM((group, 2, rows // 2, width), bf16),
            pltpu.VMEM((group,) + shares.shape, jnp.float32),
            pltpu.VMEM((pieces, width, units), bf16),
            pltpu.VMEM((pieces, width, units), bf16),
            pltpu.VMEM((pieces, width, units), bf16),
            pltpu.VMEM((pieces, group * rows, units), bf16),
            pltpu.VMEM((group * rows, width), jnp.float32),
            pltpu.VMEM((2, group, 2, rows // 2, width // 2), bf16),
            pltpu.VMEM((2, group, 2, rows // 2, width // 2), bf16),
            pltpu.SemaphoreType.DMA((3, group)),
            pltpu.SemaphoreType.DMA((3, group)),
            pltpu.SemaphoreType.DMA((2, group, 2)),
            pltpu.SemaphoreType.DMA((2, group, 2)),
            pltpu.SemaphoreType.DMA((5,)),
            pltpu.SemaphoreType.DMA((7,)),
            pltpu.SemaphoreType.DMA((7,)),
        ],
        compiler_params=pltpu.CompilerParams(
            collective_id=1, has_side_effects=True, vmem_limit_bytes=VMEM_BYTES
        ),
    )(normed, carried, shares, gate, up, down, far_gate, far_up)


def weight_pieces(weights):
    pieces = [weights]
    for bit in reversed(range(lax.axis_size("tp").bit_length() - 1)):
        pieces = pieces + [
            tuple(swapped(array, "tp", bit) for array in piece) for piece in pieces
        ]
    return pieces


def local(
    queries,
    keys,
    values,
    lambdas,
    head_gain,
    w_out,
    residual_in,
    norm_gain,
    route_ids,
    route_weight,
    w_gate,
    w_up,
    w_down,
):
    sp_size, tp_size = lax.axis_size("sp"), lax.axis_size("tp")
    carried, normed, far_gate, far_up = attend(
        queries,
        keys,
        values,
        lambdas,
        head_gain,
        w_out,
        residual_in,
        norm_gain,
        w_gate.reshape(-1, w_gate.shape[-1]),
        w_up.reshape(-1, w_up.shape[-1]),
    )
    if w_gate.shape[0] == 1 and 4 <= sp_size <= 8 and tp_size == 4:
        named = lax.broadcasted_iota(jnp.int32, (sp_size, residual_in.shape[0], 2), 0)
        shares = jnp.sum(jnp.where(named == route_ids[None], route_weight[None], 0.0), axis=2)
        return expert_layer(
            normed, carried, shares, w_gate[0], w_up[0], w_down[0], far_gate, far_up
        )
    pieces = weight_pieces((w_gate, w_up, w_down))
    carried_wide = carried.astype(jnp.float32)
    dev_rows = residual_in.shape[0]
    model_width = normed.shape[1]
    experts_here = w_gate.shape[0]
    expert_count = experts_here * lax.axis_size("sp")
    capacity = max(2, 4 * dev_rows // expert_count)
    flat_ids = route_ids.reshape(-1)
    targets = flat_ids * capacity + slot_numbers(flat_ids)
    slot_ids = lax.broadcasted_iota(jnp.int32, (expert_count * capacity, dev_rows, 2), 0)
    placement_matrix = jnp.sum(
        (targets.reshape(1, dev_rows, 2) == slot_ids).astype(jnp.int32), axis=2
    ).astype(jnp.bfloat16)
    outgoing = jnp.dot(placement_matrix, normed, preferred_element_type=jnp.float32).astype(
        jnp.bfloat16
    )
    outgoing = outgoing.reshape(lax.axis_size("sp"), experts_here, capacity, model_width)
    arrived = lax.all_to_all(outgoing, "sp", split_axis=0, concat_axis=0, tiled=True)
    summed = 0.0
    for gate_piece, up_piece, down_piece in pieces:
        gate_proj = jnp.einsum("secd,edf->secf", arrived, gate_piece, preferred_element_type=jnp.float32)
        up_proj = jnp.einsum("secd,edf->secf", arrived, up_piece, preferred_element_type=jnp.float32)
        hidden = (jax.nn.silu(gate_proj) * up_proj).astype(jnp.bfloat16)
        summed = summed + jnp.einsum(
            "secf,edf->secd", hidden, down_piece, preferred_element_type=jnp.float32
        )
    returned = send_back(summed.astype(jnp.bfloat16))
    flat_back = returned.reshape(expert_count * capacity, model_width)
    picked = (
        jnp.take(flat_back, targets, axis=0).astype(jnp.float32).reshape(dev_rows, 2, model_width)
    )
    layer_out = carried_wide + jnp.sum(route_weight[..., None] * picked, axis=1)
    return layer_out.astype(jnp.bfloat16)


def solution(mesh):
    placed = (
        P("sp", "tp"),
        P("sp", "tp"),
        P("sp", "tp"),
        P("tp"),
        P(),
        P(),
        P(("sp", "tp"), None),
        P(),
        P(("sp", "tp"), None),
        P(("sp", "tp"), None),
        P("sp", None, "tp"),
        P("sp", None, "tp"),
        P("sp", None, "tp"),
    )
    return jax.shard_map(
        local, mesh=mesh, in_specs=placed, out_specs=P(("sp", "tp"), None), check_vma=False
    )
```

profile of v0, /device:TPU:0, one launch (start us, length us, event | category | flops | bytes accessed | tf_op | source)
XLA Modules:
  0.0 148.5 jit_solution(7673958669890965231)
XLA Ops:
  0.0 1.3 select_reduce_fusion.share_ref
  1.3 56.1 %attend.1 = (bf16[128,2048]{1,0:T(8,128)(2,1)}, bf16[128,2048]{1,0:T(8,128)(2,1)}, bf16[2048,256]{1,0:T(8,128)(2,1)}, bf16[2048,256]{1,0:T(8,128)(2,1)}) custom-call(bf16[512,256]{1,0:T(8,128)(2,1)} %q_ref.1, bf16[512,256]{1,0:T(8,128)(2,1)} %k_ref.1, bf16[512,256]{1,0:T(8,128)(2,1)} %v_ref.1, f32[2]{0:T(128)} %lam_ref.1, f32[1,128]{1,0:T(1,128)} %bitcast.11, ...), custom_call_target="tpu_custom_call" | custom-call | flops 49999998976 | bytes 16000000 | tf_op jit(solution)/shard_map/attend/pallas_call | solution.py:279
  57.4 89.2 %experts.1 = bf16[128,2048]{1,0:T(8,128)(2,1)} custom-call(bf16[128,2048]{1,0:T(8,128)(2,1)} %get-tuple-element.9.x_ref, bf16[128,2048]{1,0:T(8,128)(2,1)} %get-tuple-element.10.carried_ref, f32[8,128]{1,0:T(8,128)} %select_reduce_fusion.share_ref, bf16[2048,256]{1,0:T(8,128)(2,1)} %bitcast.6, bf16[2048,256]{1,0:T(8,128)(2,1)} %bitcast.8, ...), custom_call_target="tpu_custom_call" | custom-call | tf_op jit(solution)/shard_map/experts/pallas_call | solution.py:586
  146.6 1.9 %copy.17 = bf16[128,2048]{1,0:T(8,128)(2,1)} copy(bf16[128,2048]{1,0:T(8,128)(2,1)} %experts.1) | data formatting | bytes 1048576
where the time goes:
time: 149 us; the launch traced here: 148 us
  Pallas kernels  145 us (97%)
  local copies, waits for them, and re-layouts  1.88 us (1%)
    pallas_call x1, Pallas kernels, expert_layer(): pl.pallas_call(functools.partial(expert_kernel, group), name='experts', o...  89.2 us
    pallas_call x1, Pallas kernels, attend(): pl.pallas_call(functools.partial(attention_kernel, group, tp), name='atte...  56.1 us

commit v1 on v0

--- a/solution.py
+++ b/solution.py
@@ -613,6 +613,835 @@
     )(normed, carried, shares, gate, up, down, far_gate, far_up)
 
 
+def nearest_first(position, count, nth):
+    order = [
+        sorted(range(count), key=lambda other: (abs(other - here), other if 2 * here < count else -other))
+        for here in range(count)
+    ]
+    chosen = jnp.int32(order[0][nth])
+    for here in range(1, count):
+        chosen = jnp.where(position == here, order[here][nth], chosen)
+    return chosen
+
+
+class WeightFlow:
+    def __init__(self, chunks, refs, pieces, send_sems, recv_sems, load_sems):
+        gate_ref, up_ref, down_ref = refs
+        gates, ups, downs = pieces
+        me_tp, tp = lax.axis_index("tp"), lax.axis_size("tp")
+        near = me_tp + 1 - 2 * lax.rem(me_tp, 2)
+        far = lax.rem(me_tp + tp // 2, tp)
+        width = gate_ref.shape[0]
+        half, tile = width // 2, width // chunks
+        self.used = 0
+
+        def to(target, source, landing):
+            index = self.used
+            self.used += 1
+            return pltpu.make_async_remote_copy(
+                src_ref=source,
+                dst_ref=landing,
+                send_sem=send_sems.at[index],
+                recv_sem=recv_sems.at[index],
+                device_id={"tp": target},
+                device_id_type=MESH,
+            )
+
+        cuts = [(0, pl.ds(0, width)), (1, pl.ds(0, half)), (1, pl.ds(half, half))]
+        cuts += [(2, pl.ds(chunk * tile, tile)) for chunk in range(chunks)]
+        self.far = [to(far, refs[kind].at[at], pieces[kind].at[2, at]) for kind, at in cuts]
+        self.relays = [to(near, pieces[kind].at[2, at], pieces[kind].at[3, at]) for kind, at in cuts]
+        self.near = [to(near, refs[kind], pieces[kind].at[1]) for kind in range(3)]
+        self.loads = [
+            pltpu.make_async_copy(refs[kind], pieces[kind].at[0], load_sems.at[kind])
+            for kind in range(3)
+        ]
+
+    def start_far(self, phase):
+        if phase == 0:
+            for copy in self.far[:2]:
+                copy.start()
+        else:
+            for copy in self.far[2:] + self.near + self.loads:
+                copy.start()
+            for far, relay in zip(self.far[:2], self.relays[:2]):
+                far.wait_recv()
+                relay.start()
+
+    def hidden_ready(self):
+        self.far[2].wait_recv()
+        self.relays[2].start()
+        for copy in self.loads:
+            copy.wait()
+        for copy in self.near + self.relays[:3]:
+            copy.wait_recv()
+
+    def down_ready(self, chunk):
+        self.far[3 + chunk].wait_recv()
+        self.relays[3 + chunk].start()
+        self.relays[3 + chunk].wait_recv()
+
+    def finish(self):
+        for copy in self.far + self.relays + self.near:
+            copy.wait_send()
+
+
+def attention_part(
+    sides,
+    cores,
+    start_far,
+    q_ref,
+    k_ref,
+    v_ref,
+    lam_ref,
+    gain_ref,
+    w_out_ref,
+    residual_ref,
+    norm_gain_ref,
+    carried_ref,
+    normed_ref,
+    q_here,
+    kv,
+    q_masked,
+    peaks,
+    totals,
+    numerators,
+    made,
+    came,
+    lam_all,
+    w_out_here,
+    in_send,
+    q_recv,
+    kv_recv,
+    pair_send,
+    side_send,
+    lam_sems,
+    row_send,
+    row_recv,
+    load_sems,
+):
+    rows, width = q_ref.shape
+    depth = kv.shape[2]
+    heads = width // 128
+    value_dim = width // heads
+    head_dim = value_dim // 2
+    half = rows // cores
+    exponent_scale = head_dim ** (-0.5) * math.log2(math.e)
+    me_sp, me_tp = lax.axis_index("sp"), lax.axis_index("tp")
+    tp = lax.axis_size("tp")
+    z, y = lax.div(me_sp, sides), lax.rem(me_sp, sides)
+    x, c = lax.div(me_tp, cores), lax.rem(me_tp, cores)
+    other_y, other_c = 1 - y, 1 - c
+
+    def device(at_z, at_y, at_x, at_c):
+        return {"sp": at_z * sides + at_y, "tp": at_x * cores + at_c}
+
+    lam_row = lax.broadcasted_iota(jnp.int32, lam_all.shape[1:], 0)
+    lam_block = jnp.zeros(lam_all.shape[1:], jnp.float32)
+    for head in range(heads):
+        lam_block = jnp.where(lam_row == head, lam_ref[head], lam_block)
+    lam_all[c] = lam_block
+
+    barrier = pltpu.get_barrier_semaphore()
+    plane = depth * tp
+    spot = z * tp + me_tp
+    for step in range(1, plane):
+        peer = lax.rem(spot + step, plane)
+        pl.semaphore_signal(
+            barrier,
+            inc=1,
+            device_id={"sp": lax.div(peer, tp) * sides + y, "tp": lax.rem(peer, tp)},
+            device_id_type=MESH,
+        )
+    pl.semaphore_signal(barrier, inc=1, device_id=device(z, other_y, x, c), device_id_type=MESH)
+    pl.semaphore_wait(barrier, plane)
+
+    def remote(source, landing, send_sem, recv_sem, target):
+        return pltpu.make_async_remote_copy(
+            src_ref=source,
+            dst_ref=landing,
+            send_sem=send_sem,
+            recv_sem=recv_sem,
+            device_id=target,
+            device_id_type=MESH,
+        )
+
+    def deliver(source, landing, send_sem, recv_sem, target, stays):
+        @pl.when(stays)
+        def _():
+            pltpu.make_async_copy(source, landing, recv_sem).start()
+
+        @pl.when(jnp.logical_not(stays))
+        def _():
+            remote(source, landing, send_sem, recv_sem, target).start()
+
+    def left(source, landing, send_sem, recv_sem, target, stays):
+        @pl.when(jnp.logical_not(stays))
+        def _():
+            remote(source, landing, send_sem, recv_sem, target).wait_send()
+
+    inputs = []
+    for head in range(heads):
+        columns = slice(head * value_dim, (head + 1) * value_dim)
+        to_z = c * heads + head
+        for core in range(cores):
+            inputs.append(
+                (
+                    q_ref.at[core * half : (core + 1) * half, columns],
+                    q_here.at[z],
+                    in_send.at[head, core],
+                    q_recv.at[z],
+                    device(to_z, y, x, core),
+                    jnp.logical_and(to_z == z, c == core),
+                )
+            )
+    for head in range(heads):
+        columns = slice(head * value_dim, (head + 1) * value_dim)
+        to_z = c * heads + head
+        for core, source in ((0, k_ref), (1, v_ref)):
+            inputs.append(
+                (
+                    source.at[:, columns],
+                    kv.at[core, y, z],
+                    in_send.at[head, cores + core],
+                    kv_recv.at[core, y, z],
+                    device(to_z, y, x, core),
+                    jnp.logical_and(to_z == z, c == core),
+                )
+            )
+    lam_copy = remote(lam_all.at[c], lam_all.at[c], lam_sems.at[0], lam_sems.at[1], device(z, y, x, other_c))
+    for item in inputs:
+        deliver(*item)
+    lam_copy.start()
+    start_far(0)
+    load_w_out = pltpu.make_async_copy(w_out_ref, w_out_here, load_sems.at[0])
+    load_w_out.start()
+
+    peaks[...] = jnp.full(peaks.shape, FLOOR_SCORE, jnp.float32)
+    totals[...] = jnp.zeros(totals.shape, jnp.float32)
+    numerators[...] = jnp.zeros(numerators.shape, jnp.float32)
+
+    def block_wait(tensor, side, at):
+        slot = kv.at[tensor, side, at]
+        remote(
+            slot, slot, pair_send.at[0, 0], kv_recv.at[tensor, side, at], device(z, other_y, x, c)
+        ).wait_recv()
+
+    def to_pair(side, at):
+        slot = kv.at[c, side, at]
+        return remote(
+            slot, slot, pair_send.at[side, at], kv_recv.at[c, side, at], device(z, y, x, other_c)
+        )
+
+    def to_side(at):
+        slot = kv.at[c, y, at]
+        return remote(
+            slot, slot, side_send.at[at], kv_recv.at[c, y, at], device(z, other_y, x, c)
+        )
+
+    def take_own(at):
+        block_wait(c, y, at)
+        to_side(at).start()
+        to_pair(y, at).start()
+
+    def take_side(at):
+        block_wait(c, other_y, at)
+        to_pair(other_y, at).start()
+
+    def absorb(side, at):
+        block_wait(other_c, side, at)
+        key_block = kv[0, side, at]
+        value_block = kv[1, side, at]
+        with_ones = jnp.concatenate([value_block, jnp.ones((rows, 128), jnp.bfloat16)], axis=1)
+        for part in range(2):
+            for begin in range(0, depth * half, half):
+                here = slice(begin, begin + half)
+                scores = lax.dot_general(
+                    q_masked[part, here],
+                    key_block,
+                    (((1,), (1,)), ((), ())),
+                    preferred_element_type=jnp.float32,
+                )
+                old_peak = peaks[part, here][:, :1]
+                new_peak = jnp.maximum(old_peak, jnp.max(scores, axis=1, keepdims=True))
+                weights = jnp.exp2((scores - new_peak) * exponent_scale)
+                shrink = jnp.exp2((old_peak - new_peak) * exponent_scale)
+                product = jnp.dot(
+                    weights.astype(jnp.bfloat16), with_ones, preferred_element_type=jnp.float32
+                )
+                numerators[part, here] = numerators[part, here] * shrink + product[:, :value_dim]
+                totals[part, here] = totals[part, here] * shrink + product[:, value_dim:]
+                peaks[part, here] = jnp.broadcast_to(new_peak, (half, 128))
+
+    take_own(z)
+    lane = lax.broadcasted_iota(jnp.int32, (half, value_dim), 1)
+    for at in range(depth):
+        remote(
+            q_here.at[at], q_here.at[at], pair_send.at[0, 0], q_recv.at[at], device(z, other_y, x, c)
+        ).wait_recv()
+        both = q_here[at]
+        here = slice(at * half, (at + 1) * half)
+        q_masked[0, here] = jnp.where(lane < head_dim, both, jnp.zeros_like(both))
+        q_masked[1, here] = jnp.where(lane >= head_dim, both, jnp.zeros_like(both))
+
+    def nth(index):
+        chosen = nearest_first(z, depth, 0)
+        for place in range(1, depth):
+            chosen = jnp.where(index == place, nearest_first(z, depth, place), chosen)
+        return chosen
+
+    def one_block(index, unused):
+        at = nth(index)
+        absorb(y, at)
+        take_side(at)
+
+        @pl.when(index < depth - 1)
+        def _():
+            take_own(nth(index + 1))
+
+        absorb(other_y, at)
+        return unused
+
+    lax.fori_loop(0, depth, one_block, 0)
+
+    lam_copy.wait_recv()
+    lam_here = lam_all[lax.div(z, heads)]
+    lam = jnp.sum(jnp.where(lam_row == lax.rem(z, heads), lam_here, 0.0), axis=0, keepdims=True)
+    gain = gain_ref[...] * OUT_SCALE
+    dev_rows = residual_ref.shape[0]
+    my_head = x * depth + z
+
+    def row_item(at, part):
+        return (
+            made.at[at, part * dev_rows : (part + 1) * dev_rows],
+            came.at[my_head],
+            row_send.at[at, part],
+            row_recv.at[my_head],
+            device(at, y, c, part),
+            jnp.logical_and(at == z, jnp.logical_and(x == c, c == part)),
+        )
+
+    for place in reversed(range(depth)):
+        at = nearest_first(z, depth, place)
+        here = pl.ds(pl.multiple_of(at * half, half), half)
+        first = numerators[0, here] / totals[0, here][:, :1]
+        second = numerators[1, here] / totals[1, here][:, :1]
+        combined = first - lam * second
+        mean_square = jnp.mean(combined * combined, axis=1, keepdims=True)
+        made[at] = (combined * lax.rsqrt(mean_square + EPSILON) * gain).astype(jnp.bfloat16)
+        for part in range(half // dev_rows):
+            deliver(*row_item(at, part))
+    start_far(1)
+    load_w_out.wait()
+    for head in range(came.shape[0]):
+        remote(
+            came.at[head], came.at[head], pair_send.at[0, 0], row_recv.at[head], device(z, other_y, x, c)
+        ).wait_recv()
+    attended = jnp.concatenate([came[head] for head in range(came.shape[0])], axis=1)
+    mixed = jnp.dot(attended, w_out_here[...], preferred_element_type=jnp.float32).astype(
+        jnp.bfloat16
+    )
+    carried = (residual_ref[...].astype(jnp.float32) + mixed.astype(jnp.float32)).astype(
+        jnp.bfloat16
+    )
+    carried_ref[...] = carried
+    wide = carried.astype(jnp.float32)
+    spread = jnp.mean(wide * wide, axis=1, keepdims=True)
+    normed_ref[...] = (wide * lax.rsqrt(spread + EPSILON) * norm_gain_ref[...]).astype(
+        jnp.bfloat16
+    )
+
+    def finish():
+        for item in inputs:
+            left(*item)
+        lam_copy.wait_send()
+        for at in range(depth):
+            to_side(at).wait_send()
+            to_pair(0, at).wait_send()
+            to_pair(1, at).wait_send()
+            for part in range(half // dev_rows):
+                left(*row_item(at, part))
+
+    return finish
+
+
+def expert_part(
+    sides,
+    weights,
+    x_ref,
+    carried_ref,
+    share_ref,
+    out_ref,
+    x_all,
+    share_all,
+    selections,
+    columns,
+    picked,
+    packed_out,
+    gates,
+    ups,
+    downs,
+    hidden,
+    results_out,
+    results_in,
+    results_own,
+    parts,
+    sums_in,
+    sums_out,
+    x_send,
+    x_recv,
+    share_send,
+    share_recv,
+    pack_send,
+    pack_recv,
+    result_send,
+    result_recv,
+    sum_send,
+    sum_recv,
+):
+    rows, width = x_ref.shape
+    depth = x_all.shape[0]
+    capacity = rows // 2
+    pieces = gates.shape[0]
+    chunks = x_recv.shape[1]
+    tile = width // chunks
+    me_sp, me_tp = lax.axis_index("sp"), lax.axis_index("tp")
+    z, y = lax.div(me_sp, sides), lax.rem(me_sp, sides)
+    partner = z * sides + 1 - y
+    has_below, has_above = z > 0, z < depth - 1
+    middle = jnp.logical_and(has_below, has_above)
+    blocks = [nearest_first(z, depth, place) for place in range(depth)]
+
+    def remote(source, landing, send_sem, recv_sem, target):
+        return pltpu.make_async_remote_copy(
+            src_ref=source,
+            dst_ref=landing,
+            send_sem=send_sem,
+            recv_sem=recv_sem,
+            device_id=target,
+            device_id_type=MESH,
+        )
+
+    below, above = {"sp": me_sp - sides}, {"sp": me_sp + sides}
+
+    def cut(chunk):
+        return pl.ds(chunk * tile, tile)
+
+    def x_copy(source, block, chunk, downward):
+        return remote(
+            source.at[:, cut(chunk)],
+            x_all.at[block, :, cut(chunk)],
+            x_send.at[downward, block, chunk],
+            x_recv.at[block, chunk],
+            below if downward else above,
+        )
+
+    def share_copy(source, block, downward):
+        return remote(
+            source,
+            share_all.at[block],
+            share_send.at[downward, block],
+            share_recv.at[block],
+            below if downward else above,
+        )
+
+    for downward, exists in ((0, has_above), (1, has_below)):
+
+        @pl.when(exists)
+        def _():
+            share_copy(share_ref, z, downward).start()
+            for chunk in range(chunks):
+                x_copy(x_ref, z, chunk, downward).start()
+
+    def to_far(index, source, landing):
+        return remote(source, landing, weight_send.at[index], weight_recv.at[index], {"tp": far})
+
+    def to_near(index, source, landing):
+        return remote(source, landing, weight_send.at[index], weight_recv.at[index], {"tp": near})
+
+    def select(step, share):
+        named = (share > 0.0).astype(jnp.float32)
+        earlier = lax.broadcasted_iota(jnp.int32, (rows, rows), 0) < lax.broadcasted_iota(
+            jnp.int32, (rows, rows), 1
+        )
+        rank = jnp.dot(
+            named.astype(jnp.bfloat16),
+            earlier.astype(jnp.float32).astype(jnp.bfloat16),
+            preferred_element_type=jnp.float32,
+        )
+        expert_row = lax.broadcasted_iota(jnp.int32, share.shape, 0)
+        slot = lax.broadcasted_iota(jnp.int32, (capacity, rows), 0).astype(jnp.float32)
+        diagonal = lax.broadcasted_iota(jnp.int32, (rows, rows), 0) == lax.broadcasted_iota(
+            jnp.int32, (rows, rows), 1
+        )
+        found = []
+        for side, expert in enumerate((partner, me_sp)):
+
+            def line(table):
+                return jnp.sum(jnp.where(expert_row == expert, table, 0.0), axis=0, keepdims=True)
+
+            taken = jnp.where(jnp.logical_and(slot == line(rank), line(named) > 0.0), 1.0, 0.0)
+            found.append(taken)
+            selections[step, side] = taken.T.astype(jnp.bfloat16)
+            square = jnp.where(diagonal, jnp.broadcast_to(line(share), (rows, rows)), 0.0)
+            columns[step, side] = jnp.broadcast_to(
+                jnp.sum(square, axis=1, keepdims=True), (rows, 128)
+            )
+        return jnp.concatenate(found, axis=0).astype(jnp.bfloat16)
+
+    def pack_copy(step, chunk):
+        return remote(
+            packed_out.at[step, :, cut(chunk)],
+            picked.at[pl.ds(step * rows, capacity), cut(chunk)],
+            pack_send.at[step, chunk],
+            pack_recv.at[step, chunk],
+            {"sp": partner},
+        )
+
+    def pack(step, take, chunk):
+        block = x_ref[:, cut(chunk)] if step == 0 else x_all[blocks[step], :, cut(chunk)]
+        compact = jnp.dot(take, block, preferred_element_type=jnp.float32).astype(jnp.bfloat16)
+        packed_out[step, :, cut(chunk)] = compact[:capacity]
+        picked[step * rows + capacity : (step + 1) * rows, cut(chunk)] = compact[capacity:]
+        pack_copy(step, chunk).start()
+
+    def forward(step, chunk):
+        block = blocks[step]
+        go_up = jnp.logical_and(block < z, has_above)
+        go_down = jnp.logical_and(block > z, has_below)
+        if chunk == 0:
+            share_copy(share_all.at[block], block, 0).wait_recv()
+        x_copy(x_all.at[block], block, chunk, 0).wait_recv()
+        for downward, goes in ((0, go_up), (1, go_down)):
+
+            @pl.when(goes)
+            def _():
+                if chunk == 0:
+                    share_copy(share_all.at[block], block, downward).start()
+                x_copy(x_all.at[block], block, chunk, downward).start()
+
+    def chosen(step):
+        return select(step, share_ref[...] if step == 0 else share_all[blocks[step]])
+
+    def pack_all(step):
+        take = chosen(step)
+        for chunk in range(chunks):
+            pack(step, take, chunk)
+
+    def bring(step):
+        forward(step, 0)
+        take = chosen(step)
+        pack(step, take, 0)
+        for chunk in range(1, chunks):
+            forward(step, chunk)
+            pack(step, take, chunk)
+
+    def make_hidden(first, last, piece):
+        here = slice(first * rows, last * rows)
+        x = picked[here]
+        gate_proj = jnp.dot(x, gates[piece], preferred_element_type=jnp.float32)
+        up_proj = jnp.dot(x, ups[piece], preferred_element_type=jnp.float32)
+        silu = gate_proj / (1.0 + jnp.exp(-gate_proj))
+        hidden[piece, here] = (silu * up_proj).astype(jnp.bfloat16)
+
+    def result_copy(step, chunk):
+        return remote(
+            results_out.at[step, :, cut(chunk)],
+            results_in.at[step, :, cut(chunk)],
+            result_send.at[step, chunk],
+            result_recv.at[step, chunk],
+            {"sp": partner},
+        )
+
+    def make_results(first, last, chunk):
+        total = jnp.zeros(((last - first) * rows, tile), jnp.float32)
+        for piece in range(pieces):
+            total = total + lax.dot_general(
+                hidden[piece, first * rows : last * rows],
+                downs[piece, cut(chunk)],
+                (((1,), (1,)), ((), ())),
+                preferred_element_type=jnp.float32,
+            )
+        total = total.astype(jnp.bfloat16)
+        for step in range(first, last):
+            at = (step - first) * rows
+            results_out[step, :, cut(chunk)] = total[at : at + capacity]
+            results_own[step, :, cut(chunk)] = total[at + capacity : at + rows]
+            result_copy(step, chunk).start()
+
+    def spread(step, chunk):
+        result_copy(step, chunk).wait_recv()
+        theirs = jnp.dot(
+            selections[step, 0], results_in[step, :, cut(chunk)], preferred_element_type=jnp.float32
+        )
+        ours = jnp.dot(
+            selections[step, 1], results_own[step, :, cut(chunk)], preferred_element_type=jnp.float32
+        )
+        parts[step, :, cut(chunk)] = theirs * columns[step, 0][:, :1] + ours * columns[step, 1][:, :1]
+
+    def sum_copy(step, chunk, downward):
+        block = blocks[step]
+        return remote(
+            sums_out.at[step, :, cut(chunk)],
+            sums_in.at[downward, block, :, cut(chunk)],
+            sum_send.at[step, chunk],
+            sum_recv.at[downward, block, chunk],
+            below if downward else above,
+        )
+
+    def pass_sum(step, chunk, has_outer):
+        block = blocks[step]
+        for downward, goes in ((0, block > z), (1, block < z)):
+
+            @pl.when(goes)
+            def _():
+                value = parts[step, :, cut(chunk)]
+                if has_outer:
+                    sum_copy(step, chunk, downward).wait_recv()
+                    value = value + sums_in[downward, block, :, cut(chunk)].astype(jnp.float32)
+                sums_out[step, :, cut(chunk)] = value.astype(jnp.bfloat16)
+                sum_copy(step, chunk, downward).start()
+
+    def at_end(action):
+        pl.when(jnp.logical_not(middle))(action)
+
+    def at_middle(action):
+        pl.when(middle)(action)
+
+    pack_all(0)
+    forward(1, 0)
+    first_take = chosen(1)
+    pack(1, first_take, 0)
+    at_middle(functools.partial(forward, 2, 0))
+    for chunk in range(1, chunks):
+        forward(1, chunk)
+        pack(1, first_take, chunk)
+        at_middle(functools.partial(forward, 2, chunk))
+    at_middle(functools.partial(pack_all, 2))
+
+    def packed(step):
+        for chunk in range(chunks):
+            pack_copy(step, chunk).wait_recv()
+
+    def all_hidden(step):
+        for piece in range(pieces):
+            make_hidden(step, step + 1, piece)
+
+    def settle(step, chunk):
+        spread(step, chunk)
+        at_end(functools.partial(pass_sum, step, chunk, False))
+
+    weights.hidden_ready()
+    packed(1)
+    all_hidden(1)
+    early, late = range(chunks // 2), range(chunks // 2, chunks)
+    for chunk in early:
+        weights.down_ready(chunk)
+        make_results(1, 2, chunk)
+    at_end(functools.partial(bring, 2))
+    at_middle(functools.partial(bring, 3))
+    for chunk in early:
+        settle(1, chunk)
+    packed(2)
+    all_hidden(2)
+    for chunk in early:
+        make_results(2, 3, chunk)
+    for chunk in late:
+        weights.down_ready(chunk)
+        make_results(1, 3, chunk)
+    for chunk in late:
+        settle(1, chunk)
+    packed(0)
+    all_hidden(0)
+    for chunk in range(chunks):
+        settle(2, chunk)
+    at_end(functools.partial(bring, 3))
+    packed(3)
+    all_hidden(3)
+    for chunk in range(chunks):
+        make_results(3, 4, chunk)
+    for chunk in range(chunks):
+        make_results(0, 1, chunk)
+    for chunk in range(chunks):
+        at_middle(functools.partial(pass_sum, 2, chunk, True))
+    for chunk in range(chunks):
+        spread(3, chunk)
+        at_end(functools.partial(pass_sum, 3, chunk, False))
+
+        @at_middle
+        def _():
+            pass_sum(3, chunk, True)
+            pass_sum(1, chunk, True)
+
+    for chunk in range(chunks):
+        spread(0, chunk)
+    for chunk in range(chunks):
+        here = cut(chunk)
+
+        def arrived(downward):
+            landing = sums_in.at[downward, z, :, here]
+            remote(
+                landing, landing, sum_send.at[0, chunk], sum_recv.at[downward, z, chunk], above
+            ).wait_recv()
+            parts[0, :, here] = parts[0, :, here] + sums_in[downward, z, :, here].astype(jnp.float32)
+
+        pl.when(has_below)(functools.partial(arrived, 0))
+        pl.when(has_above)(functools.partial(arrived, 1))
+        out_ref[:, here] = (carried_ref[:, here].astype(jnp.float32) + parts[0, :, here]).astype(
+            jnp.bfloat16
+        )
+
+    for downward, exists in ((0, has_above), (1, has_below)):
+
+        @pl.when(exists)
+        def _():
+            share_copy(share_ref, z, downward).wait_send()
+            for chunk in range(chunks):
+                x_copy(x_ref, z, chunk, downward).wait_send()
+
+    for step in range(1, depth):
+        block = blocks[step]
+        for downward, goes in (
+            (0, jnp.logical_and(block < z, has_above)),
+            (1, jnp.logical_and(block > z, has_below)),
+        ):
+
+            @pl.when(goes)
+            def _():
+                share_copy(share_all.at[block], block, downward).wait_send()
+                for chunk in range(chunks):
+                    x_copy(x_all.at[block], block, chunk, downward).wait_send()
+
+    for step in range(depth):
+        for chunk in range(chunks):
+            pack_copy(step, chunk).wait_send()
+            result_copy(step, chunk).wait_send()
+            if step:
+                sum_copy(step, chunk, 0).wait_send()
+
+
+def layer_kernel(sides, cores, chunks, *refs):
+    inputs, rest = refs[:8], refs[8:]
+    share_ref, gate_ref, up_ref, down_ref, out_ref = rest[:5]
+    carried, normed = rest[5:7]
+    attention_scratch, rest = rest[7:26], rest[26:]
+    expert_scratch, (weight_send, weight_recv, weight_loads) = rest[:-3], rest[-3:]
+    weights = WeightFlow(
+        chunks,
+        (gate_ref, up_ref, down_ref),
+        expert_scratch[6:9],
+        weight_send,
+        weight_recv,
+        weight_loads,
+    )
+    finish = attention_part(
+        sides, cores, weights.start_far, *inputs, carried, normed, *attention_scratch
+    )
+    expert_part(sides, weights, normed, carried, share_ref, out_ref, *expert_scratch)
+    finish()
+    weights.finish()
+
+
+def whole_layer(
+    queries, keys, values, lambdas, head_gain, w_out, residual_in, norm_gain, shares, gate, up, down
+):
+    tp = lax.axis_size("tp")
+    sides, cores, chunks = 2, 2, 4
+    depth = lax.axis_size("sp") // sides
+    rows, width = queries.shape
+    dev_rows, model_width = residual_in.shape
+    units = gate.shape[1]
+    value_dim = 128
+    heads_all = (width // value_dim) * tp
+    half = rows // cores
+    capacity = dev_rows // 2
+    vmem = pl.BlockSpec(memory_space=pltpu.VMEM)
+    smem = pl.BlockSpec(memory_space=pltpu.SMEM)
+    outside = pl.BlockSpec(memory_space=pl.ANY)
+    bf16, f32 = jnp.bfloat16, jnp.float32
+    dma = pltpu.SemaphoreType.DMA
+    attention_scratch = [
+        pltpu.VMEM((depth, half, value_dim), bf16),
+        pltpu.VMEM((2, sides, depth, rows, value_dim), bf16),
+        pltpu.VMEM((2, depth * half, value_dim), bf16),
+        pltpu.VMEM((2, depth * half, 128), f32),
+        pltpu.VMEM((2, depth * half, 128), f32),
+        pltpu.VMEM((2, depth * half, value_dim), f32),
+        pltpu.VMEM((depth, half, value_dim), bf16),
+        pltpu.VMEM((heads_all, dev_rows, value_dim), bf16),
+        pltpu.VMEM((cores, 8, 128), f32),
+        pltpu.VMEM(w_out.shape, bf16),
+        dma((width // value_dim, 2 * cores)),
+        dma((depth,)),
+        dma((2, sides, depth)),
+        dma((sides, depth)),
+        dma((depth,)),
+        dma((2,)),
+        dma((depth, half // dev_rows)),
+        dma((heads_all,)),
+        dma((1,)),
+    ]
+    expert_scratch = [
+        pltpu.VMEM((depth, dev_rows, model_width), bf16),
+        pltpu.VMEM((depth,) + shares.shape, f32),
+        pltpu.VMEM((depth, 2, dev_rows, capacity), bf16),
+        pltpu.VMEM((depth, 2, dev_rows, 128), f32),
+        pltpu.VMEM((depth * dev_rows, model_width), bf16),
+        pltpu.VMEM((depth, capacity, model_width), bf16),
+        pltpu.VMEM((tp, model_width, units), bf16),
+        pltpu.VMEM((tp, model_width, units), bf16),
+        pltpu.VMEM((tp, model_width, units), bf16),
+        pltpu.VMEM((tp, depth * dev_rows, units), bf16),
+        pltpu.VMEM((depth, capacity, model_width), bf16),
+        pltpu.VMEM((depth, capacity, model_width), bf16),
+        pltpu.VMEM((depth, capacity, model_width), bf16),
+        pltpu.VMEM((depth, dev_rows, model_width), f32),
+        pltpu.VMEM((2, depth, dev_rows, model_width), bf16),
+        pltpu.VMEM((depth, dev_rows, model_width), bf16),
+        dma((2, depth, chunks)),
+        dma((depth, chunks)),
+        dma((2, depth)),
+        dma((depth,)),
+        dma((depth, chunks)),
+        dma((depth, chunks)),
+        dma((depth, chunks)),
+        dma((depth, chunks)),
+        dma((depth, chunks)),
+        dma((2, depth, chunks)),
+    ]
+    weight_copies = 2 * (chunks + 3) + 3
+    return pl.pallas_call(
+        functools.partial(layer_kernel, sides, cores, chunks),
+        name="layer",
+        out_shape=jax.ShapeDtypeStruct((dev_rows, model_width), bf16),
+        in_specs=[vmem, vmem, vmem, smem, vmem, outside, vmem, vmem, vmem] + [outside] * 3,
+        out_specs=vmem,
+        scratch_shapes=[
+            pltpu.VMEM((dev_rows, model_width), bf16),
+            pltpu.VMEM((dev_rows, model_width), bf16),
+        ]
+        + attention_scratch
+        + expert_scratch
+        + [dma((weight_copies,)), dma((weight_copies,)), dma((3,))],
+        compiler_params=pltpu.CompilerParams(
+            collective_id=2, has_side_effects=True, vmem_limit_bytes=VMEM_BYTES
+        ),
+    )(
+        queries,
+        keys,
+        values,
+        lambdas,
+        head_gain.reshape(1, -1),
+        w_out,
+        residual_in,
+        norm_gain.reshape(1, -1),
+        shares,
+        gate,
+        up,
+        down,
+    )
+
+
 def weight_pieces(weights):
     pieces = [weights]
     for bit in reversed(range(lax.axis_size("tp").bit_length() - 1)):
@@ -638,6 +1467,14 @@
     w_down,
 ):
     sp_size, tp_size = lax.axis_size("sp"), lax.axis_size("tp")
+    whole_heads = lambdas.shape[0] * 128 == queries.shape[1]
+    square = queries.shape[0] == 2 * 2 * residual_in.shape[0]
+    columns_fit = sp_size == 8 and tp_size == 4 and lambdas.shape[0] == 2 and whole_heads and square
+    if columns_fit and w_gate.shape[0] == 1:
+        named = lax.broadcasted_iota(jnp.int32, (sp_size, residual_in.shape[0], 2), 0)
+        shares = jnp.sum(jnp.where(named == route_ids[None], route_weight[None], 0.0), axis=2)
+        tensors = (queries, keys, values, lambdas, head_gain, w_out, residual_in, norm_gain)
+        return whole_layer(*tensors, shares, w_gate[0], w_up[0], w_down[0])
     carried, normed, far_gate, far_up = attend(
         queries,
         keys,

time: 149 us -> 141 us (0.946)
  Pallas kernels: 145 us -> 138 us
    pallas_call x2 -> x1, Pallas kernels: 145 us -> 138 us  [whole_layer(): pl.pallas_call(functools.partial(layer_kernel, sides, cores, chunks), nam...]
where the time goes in v1:
time: 141 us
  Pallas kernels  138 us (98%)
  local copies, waits for them, and re-layouts  1.88 us (1%)
    pallas_call x1, Pallas kernels, whole_layer(): pl.pallas_call(functools.partial(layer_kernel, sides, cores, chunks), nam...  138 us

profile of v1, /device:TPU:0, one launch (start us, length us, event | category | flops | bytes accessed | tf_op | source)
XLA Modules:
  0.0 141.2 jit_solution(13372463036425292422)
XLA Ops:
  0.0 1.3 select_reduce_fusion.refs_8_
  1.3 138.1 %layer.1 = bf16[128,2048]{1,0:T(8,128)(2,1)} custom-call(bf16[512,256]{1,0:T(8,128)(2,1)} %refs_0_.1, bf16[512,256]{1,0:T(8,128)(2,1)} %refs_1_.1, bf16[512,256]{1,0:T(8,128)(2,1)} %refs_2_.1, f32[2]{0:T(128)} %refs_3_.1, f32[1,128]{1,0:T(1,128)} %bitcast.9, bf16[1024,2048]{1,0:T(8,128)(2,1)} %refs_5_.1, bf16[128,2048]{1,0:T(8,128)(2,1)} %refs_6_.1, ...), custom_call_target="tpu_custom_call" | custom-call | tf_op jit(solution)/shard_map/layer/pallas_call | solution.py:1413
  139.4 1.9 %copy.17 = bf16[128,2048]{1,0:T(8,128)(2,1)} copy(bf16[128,2048]{1,0:T(8,128)(2,1)} %layer.1) | data formatting | bytes 1048576

commit v2 on v1

--- a/solution.py
+++ b/solution.py
@@ -632,7 +632,7 @@
         near = me_tp + 1 - 2 * lax.rem(me_tp, 2)
         far = lax.rem(me_tp + tp // 2, tp)
         width = gate_ref.shape[0]
-        half, tile = width // 2, width // chunks
+        first, tile = width // 4, width // chunks
         self.used = 0
 
         def to(target, source, landing):
@@ -647,7 +647,7 @@
                 device_id_type=MESH,
             )
 
-        cuts = [(0, pl.ds(0, width)), (1, pl.ds(0, half)), (1, pl.ds(half, half))]
+        cuts = [(0, pl.ds(0, width)), (1, pl.ds(0, first)), (1, pl.ds(first, width - first))]
         cuts += [(2, pl.ds(chunk * tile, tile)) for chunk in range(chunks)]
         self.far = [to(far, refs[kind].at[at], pieces[kind].at[2, at]) for kind, at in cuts]
         self.relays = [to(near, pieces[kind].at[2, at], pieces[kind].at[3, at]) for kind, at in cuts]
@@ -664,9 +664,11 @@
         else:
             for copy in self.far[2:] + self.near + self.loads:
                 copy.start()
-            for far, relay in zip(self.far[:2], self.relays[:2]):
-                far.wait_recv()
-                relay.start()
+
+    def pass_first(self):
+        for far, relay in zip(self.far[:2], self.relays[:2]):
+            far.wait_recv()
+            relay.start()
 
     def hidden_ready(self):
         self.far[2].wait_recv()
@@ -848,32 +850,44 @@
         block_wait(c, other_y, at)
         to_pair(other_y, at).start()
 
-    def absorb(side, at):
-        block_wait(other_c, side, at)
-        key_block = kv[0, side, at]
-        value_block = kv[1, side, at]
-        with_ones = jnp.concatenate([value_block, jnp.ones((rows, 128), jnp.bfloat16)], axis=1)
-        for part in range(2):
-            for begin in range(0, depth * half, half):
-                here = slice(begin, begin + half)
-                scores = lax.dot_general(
-                    q_masked[part, here],
-                    key_block,
-                    (((1,), (1,)), ((), ())),
-                    preferred_element_type=jnp.float32,
-                )
-                old_peak = peaks[part, here][:, :1]
-                new_peak = jnp.maximum(old_peak, jnp.max(scores, axis=1, keepdims=True))
-                weights = jnp.exp2((scores - new_peak) * exponent_scale)
-                shrink = jnp.exp2((old_peak - new_peak) * exponent_scale)
-                product = jnp.dot(
-                    weights.astype(jnp.bfloat16), with_ones, preferred_element_type=jnp.float32
-                )
-                numerators[part, here] = numerators[part, here] * shrink + product[:, :value_dim]
-                totals[part, here] = totals[part, here] * shrink + product[:, value_dim:]
-                peaks[part, here] = jnp.broadcast_to(new_peak, (half, 128))
+    def absorb(places, part):
+        if part == 0:
+            for side, at in places:
+                block_wait(other_c, side, at)
+        key_block = jnp.concatenate([kv[0, side, at] for side, at in places], axis=0)
+        value_block = jnp.concatenate([kv[1, side, at] for side, at in places], axis=0)
+        count = len(places) * rows
+        with_ones = jnp.concatenate([value_block, jnp.ones((count, 128), jnp.bfloat16)], axis=1)
+
+        def scores_of(begin):
+            return lax.dot_general(
+                q_masked[part, begin : begin + half],
+                key_block,
+                (((1,), (1,)), ((), ())),
+                preferred_element_type=jnp.float32,
+            )
+
+        coming = scores_of(0)
+        for begin in range(0, depth * half, half):
+            here = slice(begin, begin + half)
+            scores = coming
+            if begin + half < depth * half:
+                coming = scores_of(begin + half)
+            old_peak = peaks[part, here]
+            row_peak = jnp.broadcast_to(jnp.max(scores, axis=1, keepdims=True), (half, 128))
+            new_peak = jnp.maximum(old_peak, row_peak)
+            level = jnp.concatenate([new_peak] * (count // 128), axis=1)
+            weights = jnp.exp2((scores - level) * exponent_scale)
+            shrink = jnp.exp2((old_peak - new_peak) * exponent_scale)
+            product = jnp.dot(
+                weights.astype(jnp.bfloat16), with_ones, preferred_element_type=jnp.float32
+            )
+            numerators[part, here] = numerators[part, here] * shrink + product[:, :value_dim]
+            totals[part, here] = totals[part, here] * shrink + product[:, value_dim:]
+            peaks[part, here] = new_peak
 
     take_own(z)
+    take_side(z)
     lane = lax.broadcasted_iota(jnp.int32, (half, value_dim), 1)
     for at in range(depth):
         remote(
@@ -890,19 +904,26 @@
             chosen = jnp.where(index == place, nearest_first(z, depth, place), chosen)
         return chosen
 
+    absorb([(y, z)], 0)
+    take_own(nth(1))
+    absorb([(y, z)], 1)
+
     def one_block(index, unused):
-        at = nth(index)
-        absorb(y, at)
-        take_side(at)
+        at, before = nth(index), nth(index - 1)
+        absorb([(y, at), (other_y, before)], 0)
 
         @pl.when(index < depth - 1)
         def _():
             take_own(nth(index + 1))
 
-        absorb(other_y, at)
+        take_side(at)
+        absorb([(y, at), (other_y, before)], 1)
         return unused
 
-    lax.fori_loop(0, depth, one_block, 0)
+    lax.fori_loop(1, depth, one_block, 0)
+    last = nth(depth - 1)
+    absorb([(other_y, last)], 0)
+    absorb([(other_y, last)], 1)
 
     lam_copy.wait_recv()
     lam_here = lam_all[lax.div(z, heads)]
@@ -976,6 +997,7 @@
     share_all,
     selections,
     columns,
+    takes,
     picked,
     packed_out,
     gates,
@@ -988,6 +1010,8 @@
     parts,
     sums_in,
     sums_out,
+    out_here,
+    out_sems,
     x_send,
     x_recv,
     share_send,
@@ -1005,6 +1029,8 @@
     pieces = gates.shape[0]
     chunks = x_recv.shape[1]
     tile = width // chunks
+    splits = sum_send.shape[1] // chunks
+    fine_tile = tile // splits
     me_sp, me_tp = lax.axis_index("sp"), lax.axis_index("tp")
     z, y = lax.div(me_sp, sides), lax.rem(me_sp, sides)
     partner = z * sides + 1 - y
@@ -1098,9 +1124,9 @@
             {"sp": partner},
         )
 
-    def pack(step, take, chunk):
+    def pack(step, chunk):
         block = x_ref[:, cut(chunk)] if step == 0 else x_all[blocks[step], :, cut(chunk)]
-        compact = jnp.dot(take, block, preferred_element_type=jnp.float32).astype(jnp.bfloat16)
+        compact = jnp.dot(takes[step], block, preferred_element_type=jnp.float32).astype(jnp.bfloat16)
         packed_out[step, :, cut(chunk)] = compact[:capacity]
         picked[step * rows + capacity : (step + 1) * rows, cut(chunk)] = compact[capacity:]
         pack_copy(step, chunk).start()
@@ -1120,21 +1146,19 @@
                     share_copy(share_all.at[block], block, downward).start()
                 x_copy(x_all.at[block], block, chunk, downward).start()
 
-    def chosen(step):
-        return select(step, share_ref[...] if step == 0 else share_all[blocks[step]])
+    def choose(step):
+        takes[step] = select(step, share_ref[...] if step == 0 else share_all[blocks[step]])
 
     def pack_all(step):
-        take = chosen(step)
+        choose(step)
         for chunk in range(chunks):
-            pack(step, take, chunk)
-
-    def bring(step):
-        forward(step, 0)
-        take = chosen(step)
-        pack(step, take, 0)
-        for chunk in range(1, chunks):
-            forward(step, chunk)
-            pack(step, take, chunk)
+            pack(step, chunk)
+
+    def bring(step, chunk):
+        forward(step, chunk)
+        if chunk == 0:
+            choose(step)
+        pack(step, chunk)
 
     def make_hidden(first, last, piece):
         here = slice(first * rows, last * rows)
@@ -1179,45 +1203,41 @@
         )
         parts[step, :, cut(chunk)] = theirs * columns[step, 0][:, :1] + ours * columns[step, 1][:, :1]
 
+    def fine_cut(chunk):
+        return pl.ds(chunk * fine_tile, fine_tile)
+
     def sum_copy(step, chunk, downward):
         block = blocks[step]
         return remote(
-            sums_out.at[step, :, cut(chunk)],
-            sums_in.at[downward, block, :, cut(chunk)],
+            sums_out.at[step, :, fine_cut(chunk)],
+            sums_in.at[downward, block, :, fine_cut(chunk)],
             sum_send.at[step, chunk],
             sum_recv.at[downward, block, chunk],
             below if downward else above,
         )
 
     def pass_sum(step, chunk, has_outer):
+        pass_fine(step, range(chunk * splits, (chunk + 1) * splits), has_outer)
+
+    def pass_fine(step, fines, has_outer):
         block = blocks[step]
         for downward, goes in ((0, block > z), (1, block < z)):
 
             @pl.when(goes)
             def _():
-                value = parts[step, :, cut(chunk)]
-                if has_outer:
-                    sum_copy(step, chunk, downward).wait_recv()
-                    value = value + sums_in[downward, block, :, cut(chunk)].astype(jnp.float32)
-                sums_out[step, :, cut(chunk)] = value.astype(jnp.bfloat16)
-                sum_copy(step, chunk, downward).start()
+                for fine in fines:
+                    value = parts[step, :, fine_cut(fine)]
+                    if has_outer:
+                        sum_copy(step, fine, downward).wait_recv()
+                        value = value + sums_in[downward, block, :, fine_cut(fine)].astype(jnp.float32)
+                    sums_out[step, :, fine_cut(fine)] = value.astype(jnp.bfloat16)
+                    sum_copy(step, fine, downward).start()
 
     def at_end(action):
         pl.when(jnp.logical_not(middle))(action)
 
     def at_middle(action):
         pl.when(middle)(action)
-
-    pack_all(0)
-    forward(1, 0)
-    first_take = chosen(1)
-    pack(1, first_take, 0)
-    at_middle(functools.partial(forward, 2, 0))
-    for chunk in range(1, chunks):
-        forward(1, chunk)
-        pack(1, first_take, chunk)
-        at_middle(functools.partial(forward, 2, chunk))
-    at_middle(functools.partial(pack_all, 2))
 
     def packed(step):
         for chunk in range(chunks):
@@ -1231,35 +1251,56 @@
         spread(step, chunk)
         at_end(functools.partial(pass_sum, step, chunk, False))
 
+    def second(chunk):
+        at_end(functools.partial(bring, 2, chunk))
+        at_middle(functools.partial(bring, 3, chunk))
+
+    def third(chunk):
+        at_end(functools.partial(bring, 3, chunk))
+
+    pack_all(0)
+    weights.pass_first()
+    for chunk in range(chunks):
+        bring(1, chunk)
+        at_middle(functools.partial(forward, 2, chunk))
+    at_middle(functools.partial(pack_all, 2))
     weights.hidden_ready()
+    second(0)
     packed(1)
     all_hidden(1)
-    early, late = range(chunks // 2), range(chunks // 2, chunks)
-    for chunk in early:
-        weights.down_ready(chunk)
-        make_results(1, 2, chunk)
-    at_end(functools.partial(bring, 2))
-    at_middle(functools.partial(bring, 3))
-    for chunk in early:
-        settle(1, chunk)
+    second(1)
+    weights.down_ready(0)
+    make_results(1, 2, 0)
+    second(2)
+    weights.down_ready(1)
+    make_results(1, 2, 1)
+    second(3)
+    settle(1, 0)
     packed(2)
     all_hidden(2)
-    for chunk in early:
-        make_results(2, 3, chunk)
-    for chunk in late:
-        weights.down_ready(chunk)
-        make_results(1, 3, chunk)
-    for chunk in late:
-        settle(1, chunk)
-    packed(0)
-    all_hidden(0)
-    for chunk in range(chunks):
-        settle(2, chunk)
-    at_end(functools.partial(bring, 3))
+    make_results(2, 3, 0)
+    make_results(2, 3, 1)
+    third(0)
+    settle(1, 1)
+    third(1)
+    weights.down_ready(2)
+    make_results(1, 3, 2)
+    third(2)
+    settle(2, 0)
+    settle(2, 1)
+    settle(1, 2)
+    third(3)
+    weights.down_ready(3)
+    make_results(1, 3, 3)
+    settle(2, 2)
     packed(3)
     all_hidden(3)
     for chunk in range(chunks):
         make_results(3, 4, chunk)
+    settle(1, 3)
+    settle(2, 3)
+    packed(0)
+    all_hidden(0)
     for chunk in range(chunks):
         make_results(0, 1, chunk)
     for chunk in range(chunks):
@@ -1268,28 +1309,39 @@
         spread(3, chunk)
         at_end(functools.partial(pass_sum, 3, chunk, False))
 
-        @at_middle
-        def _():
-            pass_sum(3, chunk, True)
-            pass_sum(1, chunk, True)
-
+    @at_middle
+    def _():
+        lag, fines = 3, chunks * splits
+        for fine in range(fines + lag):
+            if fine < fines:
+                pass_fine(3, (fine,), True)
+            if fine >= lag:
+                pass_fine(1, (fine - lag,), True)
+
+    stores = []
     for chunk in range(chunks):
         spread(0, chunk)
     for chunk in range(chunks):
         here = cut(chunk)
 
         def arrived(downward):
-            landing = sums_in.at[downward, z, :, here]
-            remote(
-                landing, landing, sum_send.at[0, chunk], sum_recv.at[downward, z, chunk], above
-            ).wait_recv()
-            parts[0, :, here] = parts[0, :, here] + sums_in[downward, z, :, here].astype(jnp.float32)
+            for fine in range(chunk * splits, (chunk + 1) * splits):
+                there = fine_cut(fine)
+                landing = sums_in.at[downward, z, :, there]
+                remote(
+                    landing, landing, sum_send.at[0, fine], sum_recv.at[downward, z, fine], above
+                ).wait_recv()
+                parts[0, :, there] = parts[0, :, there] + sums_in[downward, z, :, there].astype(
+                    jnp.float32
+                )
 
         pl.when(has_below)(functools.partial(arrived, 0))
         pl.when(has_above)(functools.partial(arrived, 1))
-        out_ref[:, here] = (carried_ref[:, here].astype(jnp.float32) + parts[0, :, here]).astype(
+        out_here[:, here] = (carried_ref[:, here].astype(jnp.float32) + parts[0, :, here]).astype(
             jnp.bfloat16
         )
+        stores.append(pltpu.make_async_copy(out_here.at[:, here], out_ref.at[:, here], out_sems.at[chunk]))
+        stores[-1].start()
 
     for downward, exists in ((0, has_above), (1, has_below)):
 
@@ -1316,20 +1368,30 @@
         for chunk in range(chunks):
             pack_copy(step, chunk).wait_send()
             result_copy(step, chunk).wait_send()
-            if step:
+        if step:
+            for chunk in range(chunks * splits):
                 sum_copy(step, chunk, 0).wait_send()
+
+    return stores
 
 
 def layer_kernel(sides, cores, chunks, *refs):
     inputs, rest = refs[:8], refs[8:]
-    share_ref, gate_ref, up_ref, down_ref, out_ref = rest[:5]
-    carried, normed = rest[5:7]
-    attention_scratch, rest = rest[7:26], rest[26:]
+    ids_ref, shares_ref, gate_ref, up_ref, down_ref, out_ref = rest[:6]
+    carried, normed, share_here = rest[6:9]
+    attention_scratch, rest = rest[9:28], rest[28:]
+    dev_rows, routes = ids_ref.shape
+    lane = lax.broadcasted_iota(jnp.int32, (dev_rows, 128), 1)
+    table = jnp.zeros((dev_rows, 128), jnp.float32)
+    for route in range(routes):
+        hit = ids_ref[:, route : route + 1] == lane
+        table = table + jnp.where(hit, shares_ref[:, route : route + 1], 0.0)
+    share_here[...] = table.T[: share_here.shape[0]]
     expert_scratch, (weight_send, weight_recv, weight_loads) = rest[:-3], rest[-3:]
     weights = WeightFlow(
         chunks,
         (gate_ref, up_ref, down_ref),
-        expert_scratch[6:9],
+        expert_scratch[7:10],
         weight_send,
         weight_recv,
         weight_loads,
@@ -1337,17 +1399,32 @@
     finish = attention_part(
         sides, cores, weights.start_far, *inputs, carried, normed, *attention_scratch
     )
-    expert_part(sides, weights, normed, carried, share_ref, out_ref, *expert_scratch)
+    stores = expert_part(sides, weights, normed, carried, share_here, out_ref, *expert_scratch)
     finish()
     weights.finish()
+    for copy in stores:
+        copy.wait()
 
 
 def whole_layer(
-    queries, keys, values, lambdas, head_gain, w_out, residual_in, norm_gain, shares, gate, up, down
+    queries,
+    keys,
+    values,
+    lambdas,
+    head_gain,
+    w_out,
+    residual_in,
+    norm_gain,
+    route_ids,
+    route_weight,
+    gate,
+    up,
+    down,
 ):
     tp = lax.axis_size("tp")
     sides, cores, chunks = 2, 2, 4
-    depth = lax.axis_size("sp") // sides
+    experts = lax.axis_size("sp")
+    depth = experts // sides
     rows, width = queries.shape
     dev_rows, model_width = residual_in.shape
     units = gate.shape[1]
@@ -1383,9 +1460,10 @@
     ]
     expert_scratch = [
         pltpu.VMEM((depth, dev_rows, model_width), bf16),
-        pltpu.VMEM((depth,) + shares.shape, f32),
+        pltpu.VMEM((depth, experts, dev_rows), f32),
         pltpu.VMEM((depth, 2, dev_rows, capacity), bf16),
         pltpu.VMEM((depth, 2, dev_rows, 128), f32),
+        pltpu.VMEM((depth, dev_rows, dev_rows), bf16),
         pltpu.VMEM((depth * dev_rows, model_width), bf16),
         pltpu.VMEM((depth, capacity, model_width), bf16),
         pltpu.VMEM((tp, model_width, units), bf16),
@@ -1398,6 +1476,8 @@
         pltpu.VMEM((depth, dev_rows, model_width), f32),
         pltpu.VMEM((2, depth, dev_rows, model_width), bf16),
         pltpu.VMEM((depth, dev_rows, model_width), bf16),
+        pltpu.VMEM((dev_rows, model_width), bf16),
+        dma((chunks,)),
         dma((2, depth, chunks)),
         dma((depth, chunks)),
         dma((2, depth)),
@@ -1406,19 +1486,20 @@
         dma((depth, chunks)),
         dma((depth, chunks)),
         dma((depth, chunks)),
-        dma((depth, chunks)),
-        dma((2, depth, chunks)),
+        dma((depth, 2 * chunks)),
+        dma((2, depth, 2 * chunks)),
     ]
     weight_copies = 2 * (chunks + 3) + 3
     return pl.pallas_call(
         functools.partial(layer_kernel, sides, cores, chunks),
         name="layer",
         out_shape=jax.ShapeDtypeStruct((dev_rows, model_width), bf16),
-        in_specs=[vmem, vmem, vmem, smem, vmem, outside, vmem, vmem, vmem] + [outside] * 3,
-        out_specs=vmem,
+        in_specs=[vmem, vmem, vmem, smem, vmem, outside] + [vmem] * 4 + [outside] * 3,
+        out_specs=outside,
         scratch_shapes=[
             pltpu.VMEM((dev_rows, model_width), bf16),
             pltpu.VMEM((dev_rows, model_width), bf16),
+            pltpu.VMEM((experts, dev_rows), f32),
         ]
         + attention_scratch
         + expert_scratch
@@ -1435,7 +1516,8 @@
         w_out,
         residual_in,
         norm_gain.reshape(1, -1),
-        shares,
+        route_ids,
+        route_weight,
         gate,
         up,
         down,
@@ -1471,10 +1553,8 @@
     square = queries.shape[0] == 2 * 2 * residual_in.shape[0]
     columns_fit = sp_size == 8 and tp_size == 4 and lambdas.shape[0] == 2 and whole_heads and square
     if columns_fit and w_gate.shape[0] == 1:
-        named = lax.broadcasted_iota(jnp.int32, (sp_size, residual_in.shape[0], 2), 0)
-        shares = jnp.sum(jnp.where(named == route_ids[None], route_weight[None], 0.0), axis=2)
         tensors = (queries, keys, values, lambdas, head_gain, w_out, residual_in, norm_gain)
-        return whole_layer(*tensors, shares, w_gate[0], w_up[0], w_down[0])
+        return whole_layer(*tensors, route_ids, route_weight, w_gate[0], w_up[0], w_down[0])
     carried, normed, far_gate, far_up = attend(
         queries,
         keys,

time: 141 us -> 129 us (0.915)
  Pallas kernels: 138 us -> 124 us
  local copies, waits for them, and re-layouts: 1.88 us -> 4.7 us
    pallas_call x1, Pallas kernels: 138 us -> 124 us  [whole_layer(): pl.pallas_call(functools.partial(layer_kernel, sides, cores, chunks), nam...]
    unnamed x1 -> x3, local copies, waits for them, and re-layouts: 1.88 us -> 4.7 us
where the time goes in v2:
time: 129 us; the launch traced here: 128 us
  Pallas kernels  124 us (96%)
  local copies, waits for them, and re-layouts  4.7 us (4%)
    pallas_call x1, Pallas kernels, whole_layer(): pl.pallas_call(functools.partial(layer_kernel, sides, cores, chunks), nam...  124 us
    unnamed x3, local copies, waits for them, and re-layouts  4.7 us

profile of v2, /device:TPU:0, one launch (start us, length us, event | category | flops | bytes accessed | tf_op | source)
XLA Modules:
  0.0 128.3 jit_solution(3929183586652633461)
XLA Ops:
  0.0 1.4 %copy.14.refs_8_ = s32[128,2]{1,0:T(8,128)} copy(s32[128,2]{0,1:T(2,128)} %param.21) | data formatting | bytes 2048 | tf_op args[8]
  1.4 1.4 %copy.15.refs_9_ = f32[128,2]{1,0:T(8,128)} copy(f32[128,2]{0,1:T(2,128)} %param.22) | data formatting | bytes 2048 | tf_op args[9]
  2.8 123.6 %layer.1 = bf16[128,2048]{1,0:T(8,128)(2,1)} custom-call(bf16[512,256]{1,0:T(8,128)(2,1)} %refs_0_.1, bf16[512,256]{1,0:T(8,128)(2,1)} %refs_1_.1, bf16[512,256]{1,0:T(8,128)(2,1)} %refs_2_.1, f32[2]{0:T(128)} %refs_3_.1, f32[1,128]{1,0:T(1,128)} %bitcast.9, bf16[1024,2048]{1,0:T(8,128)(2,1)} %refs_5_.1, bf16[128,2048]{1,0:T(8,128)(2,1)} %refs_6_.1, ...), custom_call_target="tpu_custom_call" | custom-call | tf_op jit(solution)/shard_map/layer/pallas_call | solution.py:1493
  126.4 1.9 %copy.17 = bf16[128,2048]{1,0:T(8,128)(2,1)} copy(bf16[128,2048]{1,0:T(8,128)(2,1)} %layer.1) | data formatting | bytes 1048576

commit v3 on v2

--- a/solution.py
+++ b/solution.py
@@ -632,7 +632,7 @@
         near = me_tp + 1 - 2 * lax.rem(me_tp, 2)
         far = lax.rem(me_tp + tp // 2, tp)
         width = gate_ref.shape[0]
-        first, tile = width // 4, width // chunks
+        first, tile = 3 * width // 8, width // chunks
         self.used = 0
 
         def to(target, source, landing):
@@ -712,6 +712,7 @@
     came,
     lam_all,
     w_out_here,
+    residual_here,
     in_send,
     q_recv,
     kv_recv,
@@ -818,6 +819,8 @@
     start_far(0)
     load_w_out = pltpu.make_async_copy(w_out_ref, w_out_here, load_sems.at[0])
     load_w_out.start()
+    load_residual = pltpu.make_async_copy(residual_ref, residual_here, load_sems.at[1])
+    load_residual.start()
 
     peaks[...] = jnp.full(peaks.shape, FLOOR_SCORE, jnp.float32)
     totals[...] = jnp.zeros(totals.shape, jnp.float32)
@@ -954,6 +957,7 @@
             deliver(*row_item(at, part))
     start_far(1)
     load_w_out.wait()
+    load_residual.wait()
     for head in range(came.shape[0]):
         remote(
             came.at[head], came.at[head], pair_send.at[0, 0], row_recv.at[head], device(z, other_y, x, c)
@@ -962,7 +966,7 @@
     mixed = jnp.dot(attended, w_out_here[...], preferred_element_type=jnp.float32).astype(
         jnp.bfloat16
     )
-    carried = (residual_ref[...].astype(jnp.float32) + mixed.astype(jnp.float32)).astype(
+    carried = (residual_here[...].astype(jnp.float32) + mixed.astype(jnp.float32)).astype(
         jnp.bfloat16
     )
     carried_ref[...] = carried
@@ -1288,10 +1292,10 @@
     third(2)
     settle(2, 0)
     settle(2, 1)
-    settle(1, 2)
     third(3)
     weights.down_ready(3)
     make_results(1, 3, 3)
+    settle(1, 2)
     settle(2, 2)
     packed(3)
     all_hidden(3)
@@ -1299,15 +1303,19 @@
         make_results(3, 4, chunk)
     settle(1, 3)
     settle(2, 3)
-    packed(0)
-    all_hidden(0)
-    for chunk in range(chunks):
-        make_results(0, 1, chunk)
+    def finish_own():
+        packed(0)
+        all_hidden(0)
+        for chunk in range(chunks):
+            make_results(0, 1, chunk)
+
+    at_middle(finish_own)
     for chunk in range(chunks):
         at_middle(functools.partial(pass_sum, 2, chunk, True))
     for chunk in range(chunks):
         spread(3, chunk)
         at_end(functools.partial(pass_sum, 3, chunk, False))
+    at_end(finish_own)
 
     @at_middle
     def _():
@@ -1379,7 +1387,7 @@
     inputs, rest = refs[:8], refs[8:]
     ids_ref, shares_ref, gate_ref, up_ref, down_ref, out_ref = rest[:6]
     carried, normed, share_here = rest[6:9]
-    attention_scratch, rest = rest[9:28], rest[28:]
+    attention_scratch, rest = rest[9:29], rest[29:]
     dev_rows, routes = ids_ref.shape
     lane = lax.broadcasted_iota(jnp.int32, (dev_rows, 128), 1)
     table = jnp.zeros((dev_rows, 128), jnp.float32)
@@ -1448,6 +1456,7 @@
         pltpu.VMEM((heads_all, dev_rows, value_dim), bf16),
         pltpu.VMEM((cores, 8, 128), f32),
         pltpu.VMEM(w_out.shape, bf16),
+        pltpu.VMEM(residual_in.shape, bf16),
         dma((width // value_dim, 2 * cores)),
         dma((depth,)),
         dma((2, sides, depth)),
@@ -1456,7 +1465,7 @@
         dma((2,)),
         dma((depth, half // dev_rows)),
         dma((heads_all,)),
-        dma((1,)),
+        dma((2,)),
     ]
     expert_scratch = [
         pltpu.VMEM((depth, dev_rows, model_width), bf16),
@@ -1494,7 +1503,7 @@
         functools.partial(layer_kernel, sides, cores, chunks),
         name="layer",
         out_shape=jax.ShapeDtypeStruct((dev_rows, model_width), bf16),
-        in_specs=[vmem, vmem, vmem, smem, vmem, outside] + [vmem] * 4 + [outside] * 3,
+        in_specs=[outside] * 3 + [smem, vmem, outside, outside] + [vmem] * 3 + [outside] * 3,
         out_specs=outside,
         scratch_shapes=[
             pltpu.VMEM((dev_rows, model_width), bf16),

time: 129 us -> 128 us (level)
  no operation moved by 1% of the time
where the time goes in v3:
time: 128 us
  Pallas kernels  123 us (96%)
  local copies, waits for them, and re-layouts  4.7 us (4%)
    pallas_call x1, Pallas kernels, whole_layer(): pl.pallas_call(functools.partial(layer_kernel, sides, cores, chunks), nam...  123 us
    unnamed x3, local copies, waits for them, and re-layouts  4.7 us

profile of v3, /device:TPU:0, one launch (start us, length us, event | category | flops | bytes accessed | tf_op | source)
XLA Modules:
  0.0 127.7 jit_solution(5812895287871147571)
XLA Ops:
  0.0 1.4 %copy.14.refs_8_ = s32[128,2]{1,0:T(8,128)} copy(s32[128,2]{0,1:T(2,128)} %param.21) | data formatting | bytes 2048 | tf_op args[8]
  1.4 1.4 %copy.15.refs_9_ = f32[128,2]{1,0:T(8,128)} copy(f32[128,2]{0,1:T(2,128)} %param.22) | data formatting | bytes 2048 | tf_op args[9]
  2.8 123.0 %layer.1 = bf16[128,2048]{1,0:T(8,128)(2,1)} custom-call(bf16[512,256]{1,0:T(8,128)(2,1)} %refs_0_.1, bf16[512,256]{1,0:T(8,128)(2,1)} %refs_1_.1, bf16[512,256]{1,0:T(8,128)(2,1)} %refs_2_.1, f32[2]{0:T(128)} %refs_3_.1, f32[1,128]{1,0:T(1,128)} %bitcast.9, bf16[1024,2048]{1,0:T(8,128)(2,1)} %refs_5_.1, bf16[128,2048]{1,0:T(8,128)(2,1)} %refs_6_.1, ...), custom_call_target="tpu_custom_call" | custom-call | tf_op jit(solution)/shard_map/layer/pallas_call | solution.py:1502
  125.9 1.9 %copy.17 = bf16[128,2048]{1,0:T(8,128)(2,1)} copy(bf16[128,2048]{1,0:T(8,128)(2,1)} %layer.1) | data formatting | bytes 1048576
